TPU v7x, 32 devices: a whole 2x2x4 slice. The times are simulated.
32 devices in a mesh: grp: 2 (over y), sp: 4 (over z), tp: 4 (over x, core).
Axes of the slice: x: 2, y: 2, z: 4, core: 2. Of those that a mesh axis runs over, the one named last changes fastest.
Arguments:
- tokens: bfloat16 [1024, 2048], P(('grp', 'sp'), 'tp'), parts along dimension 0, may hold values from -30 to 30, as said below
- norm_gain: float32 [2, 2048], replicated, may hold values from 0.1 to 1.9
- in_weight: bfloat16 [2, 2048, 2048], P(None, 'sp', 'tp'), may hold values from -0.125 to 0.125
- gate_weight: bfloat16 [2, 2048, 2048], P(None, 'sp', 'tp'), may hold values from -0.125 to 0.125
- conv_taps: float32 [2, 4, 2048], P(None, None, 'tp'), may hold values from -3 to 3
- decay_logit: float32 [2, 2, 2048], P(None, None, 'tp'), may hold values from 4 to 20, as said below
- gate_maps: bfloat16 [2, 2048, 1024], P(None, 'tp', 'sp'), may hold values from -0.375 to 0.375
- out_weight: bfloat16 [2, 2048, 2048], P(None, 'sp', 'tp'), may hold values from -0.375 to 0.375
- final_gain: float32 [2048], P('tp'), may hold values from 0.1 to 1.9
Outputs:
- normed_out: bfloat16 [1024, 2048], P(('grp', 'sp'), 'tp'), parts along dimension 0
There are 2 independent parts, one for each index of `grp`. A program takes and returns all parts, laid end to end along the dimension named above; an argument that names none is the same for every part. Nothing has to cross between parts.
Inputs may be any that keep to these rules, and one draw needn't show every extreme that they name: Activations of order one whose scale changes by blocks of tokens and of channels. `decay_logit`: decay parameters; channels differ in how far their state reaches.
All inputs are finite; a program needn't handle non-finite values.
Results may differ from a plain program's by a relative error of at most 0.02.
Values may be sent and summed in bfloat16 or wider, within the bound.
A program may use at most 128 MiB of HBM per device.

v0:
```python
import jax
import jax.numpy as jnp
from jax import lax
from jax.experimental import pallas as pl
from jax.experimental.pallas import tpu as pltpu
from jax.sharding import PartitionSpec as P

D = 2048
HEAD_W = 256
TAPS = 4
LAYERS = 2


EPS = 1e-06


def extended(value, sides, width):
    for axis, dim in sides:
        devices, length = (lax.axis_size(axis), value.shape[dim])
        up = [(i, (i + 1) % devices) for i in range(devices - 1)]
        down = [(j, i) for i, j in up]
        last = lax.slice_in_dim(value, length - width, length, axis=dim)
        leading = lax.slice_in_dim(value, 0, width, axis=dim)
        before = lax.ppermute(last, axis, up)
        after = lax.ppermute(leading, axis, down)
        value = jnp.concatenate([before, value, after], axis=dim)
    return value


def combine_pair(earlier, later):
    return (earlier[0] * later[0], later[0] * earlier[1] + later[1])


def body(
    tokens,
    norm_gain,
    in_weight,
    gate_weight,
    conv_taps,
    decay_logit,
    gate_maps,
    out_weight,
    final_gain,
):
    resid = tokens
    rows = tokens.shape[0]
    width = in_weight.shape[2]
    local_heads = width // HEAD_W
    for layer in range(LAYERS):
        whole = lax.all_gather(resid, "tp", axis=1, tiled=True)
        wide = whole.astype(jnp.float32)
        normed = (
            wide * lax.rsqrt(jnp.mean(wide * wide, axis=1, keepdims=True) + EPS) * norm_gain[layer]
        ).astype(jnp.bfloat16)
        proj_in = jnp.dot(
            normed,
            lax.all_gather(in_weight[layer], "sp", axis=0, tiled=True),
            preferred_element_type=jnp.float32,
        )
        proj_gate = jnp.dot(
            normed,
            lax.all_gather(gate_weight[layer], "sp", axis=0, tiled=True),
            preferred_element_type=jnp.float32,
        )
        xin = proj_in.astype(jnp.bfloat16)
        gin = proj_gate.astype(jnp.bfloat16)
        padded = extended(xin, (("sp", 0),), 2).astype(jnp.float32)
        conv = conv_taps[layer, 0] * padded[0:rows]
        for k in range(1, TAPS):
            conv = conv + conv_taps[layer, k] * padded[k : k + rows]
        conv = conv.astype(jnp.bfloat16)
        stacked = conv.reshape(rows, local_heads, HEAD_W)
        piece = lax.all_gather(gate_maps[layer], "sp", axis=1, tiled=True)
        blocks = piece.reshape(local_heads, HEAD_W, piece.shape[1])
        pre = jnp.einsum("thi,hij->thj", stacked, blocks, preferred_element_type=jnp.float32)
        pre = pre.reshape(rows, local_heads, 4, HEAD_W)
        conv32 = conv.astype(jnp.float32)
        locals_a = []
        locals_h = []
        for direction in range(2):
            rate = jax.nn.sigmoid(pre[:, :, 2 * direction]).reshape(rows, width)
            inp = jax.nn.sigmoid(pre[:, :, 2 * direction + 1]).reshape(rows, width)
            log_a = -8.0 * rate * jax.nn.softplus(-decay_logit[layer, direction])
            decay = jnp.exp(log_a)
            drive = jnp.sqrt(-jnp.expm1(2.0 * log_a)) * inp * conv32
            prod_a, state = lax.associative_scan(
                combine_pair, (decay, drive), reverse=direction == 1, axis=0
            )
            locals_a.append(prod_a)
            locals_h.append(state)
        summary = jnp.stack([locals_a[0][-1], locals_h[0][-1], locals_a[1][0], locals_h[1][0]])[
            None
        ]
        every = lax.all_gather(summary, "sp", axis=0, tiled=True)
        count = every.shape[0]
        me = lax.axis_index("sp")
        _, incl_f = lax.associative_scan(combine_pair, (every[:, 0], every[:, 1]), axis=0)
        _, incl_b = lax.associative_scan(
            combine_pair, (every[:, 2], every[:, 3]), reverse=True, axis=0
        )
        before = lax.dynamic_index_in_dim(incl_f, jnp.maximum(me - 1, 0), 0, keepdims=False)
        after = lax.dynamic_index_in_dim(incl_b, jnp.minimum(me + 1, count - 1), 0, keepdims=False)
        carry_f = before * (me > 0).astype(jnp.float32)
        carry_b = after * (me < count - 1).astype(jnp.float32)
        hidden = locals_h[0] + locals_a[0] * carry_f + locals_h[1] + locals_a[1] * carry_b
        mix = (jax.nn.gelu(gin.astype(jnp.float32)) * hidden).astype(jnp.bfloat16)
        full_mix = lax.all_gather(mix, "tp", axis=1, tiled=True)
        out = jnp.dot(
            full_mix,
            lax.all_gather(out_weight[layer], "sp", axis=0, tiled=True),
            preferred_element_type=jnp.float32,
        )
        resid = (resid.astype(jnp.float32) + out).astype(jnp.bfloat16)
    wide = resid.astype(jnp.float32)
    total = lax.psum(jnp.sum(wide * wide, axis=1), "tp")
    scale = lax.rsqrt(total / D + EPS)
    return (wide * scale[:, None] * final_gain).astype(jnp.bfloat16)


LANES = 128
UNITS = 4
TILE = 256
BF16 = jnp.bfloat16
F32 = jnp.float32


def shifted(value, k, fill, reverse):
    pad = jnp.full((k, value.shape[1]), fill, value.dtype)
    if reverse:
        return jnp.concatenate([value[k:], pad], axis=0)
    return jnp.concatenate([pad, value[:-k]], axis=0)


def scan_rows(decay, state, reverse):
    k, rows = 1, decay.shape[0]
    while k < rows:
        state = state + decay * shifted(state, k, 0.0, reverse)
        if 2 * k < rows:
            decay = decay * shifted(decay, k, 1.0, reverse)
        k *= 2
    return state


def one_minus_exp_neg(u):
    series = u * (1 - u / 2 * (1 - u / 3 * (1 - u / 4 * (1 - u / 5 * (1 - u / 6 * (1 - u / 7))))))
    return jnp.where(u < 0.3, series, 1.0 - jnp.exp(-u))


def kernel(
    S,
    T,
    tok_ref,
    gain_ref,
    in_ref,
    gate_ref,
    taps_ref,
    logit_ref,
    map_ref,
    outw_ref,
    fgain_ref,
    out_ref,
    full,
    normed,
    wbuf,
    obuf,
    mbuf,
    tapb,
    logb,
    proj,
    padded,
    convb,
    fin,
    ssq,
    wss,
    wrs,
    yss,
    yrs,
    zss,
    zrs,
    xss,
    xrs,
    css,
    crs,
    vss,
    vrs,
    pss,
    prs,
    fss,
    frs,
    qss,
    qrs,
    lsem,
):
    g = lax.axis_index("grp")
    s = lax.axis_index("sp")
    t = lax.axis_index("tp")
    c = t % 2
    tc = t + 1 - 2 * c
    tx = (t + 2) % T
    rows, tcols = tok_ref.shape
    tokens = rows * S
    half = in_ref.shape[1] // 2

    def slice_of(ss, tt):
        return 2 * (S * (tt // 2) + ss) + tt % 2

    def lanes(i):
        return pl.ds(pl.multiple_of(i * LANES, LANES), LANES)

    mine = slice_of(s, t)
    home = mine // T
    sub = mine % T

    def owner(q):
        j = T * t + q
        return (j // 2) % S, 2 * (j // (2 * S)) + j % 2

    barrier = pltpu.get_barrier_semaphore()
    for ds in range(S):
        for dt in range(T):
            if ds or dt:
                pl.semaphore_signal(
                    barrier,
                    inc=1,
                    device_id={"sp": (s + ds) % S, "tp": (t + dt) % T},
                    device_id_type=pl.DeviceIdType.MESH,
                )
    pl.semaphore_signal(
        barrier, inc=1, device_id={"grp": 1 - g}, device_id_type=pl.DeviceIdType.MESH
    )
    pl.semaphore_wait(barrier, S * T)

    def remote(src, dst, ssem, rsem, dev):
        return pltpu.make_async_remote_copy(
            src_ref=src,
            dst_ref=dst,
            send_sem=ssem,
            recv_sem=rsem,
            device_id=dev,
            device_id_type=pl.DeviceIdType.MESH,
        )

    def wcopy(layer, kind, q, part, source, dev):
        if kind == 2:
            src = map_ref.at[
                layer, pl.ds((q // 2) * HEAD_W + part * LANES, LANES), pl.ds((q % 2) * LANES, LANES)
            ]
            dst = mbuf.at[layer, source, part]
        else:
            ref = (in_ref, gate_ref, None, outw_ref)[kind]
            src = ref.at[layer, pl.ds(part * half, half), pl.ds(q * LANES, LANES)]
            if kind == 3:
                dst = obuf.at[layer, source, part]
            else:
                dst = wbuf.at[layer, source, part, :, pl.ds(kind * LANES, LANES)]
        k = max(kind - 1, 0)
        rsem = wrs.at[layer, k, source]
        if dev is None:
            return pltpu.make_async_copy(src, dst, rsem)
        return remote(src, dst, wss.at[layer, k], rsem, {"sp": dev[0], "tp": dev[1]})

    def weights_start(layer, kinds):
        for kind in kinds:
            for q in range(T):
                ds, dt = owner(q)

                @pl.when(ds != s)
                def _():
                    wcopy(layer, kind, q, g, s, owner(q)).start()

        for kind in kinds:
            for q in range(T):
                ds, dt = owner(q)

                @pl.when(jnp.logical_and(ds == s, dt == t))
                def _():
                    for part in range(2):
                        wcopy(layer, kind, q, part, s, None).start()

                @pl.when(jnp.logical_and(ds == s, dt != t))
                def _():
                    for part in range(2):
                        wcopy(layer, kind, q, part, s, owner(q)).start()

    def bulk(ref, sem):
        pltpu.make_async_copy(ref, ref, sem).wait()

    def forward(layer, k, source):
        at = (wbuf, mbuf, obuf)[k].at[layer, source, g]
        return remote(at, at, yss.at[layer, k], yrs.at[layer, k], {"grp": 1 - g})

    def weights_forward(layer, k):
        buf = (wbuf, mbuf, obuf)[k]
        for d in (1, S - 1, *range(2, S - 1)):
            source = (s + d) % S
            bulk(buf.at[layer, source, g], wrs.at[layer, k, source])
            forward(layer, k, source).start()

    def weights_wait(layer, k):
        buf = (wbuf, mbuf, obuf)[k]
        bulk(buf.at[layer, s], wrs.at[layer, k, s])
        bulk(buf.at[layer, pl.ds(0, S - 1), 1 - g], yrs.at[layer, k])

    def weights_drain(layer, k):
        buf = (wbuf, mbuf, obuf)[k]
        bulk(buf.at[layer, pl.ds(0, T // 2)], wss.at[layer, k])
        bulk(buf.at[layer, pl.ds(0, S - 1), g], yss.at[layer, k])

    part_units = UNITS // 2
    units = UNITS + part_units

    def region(gi, ss, tt, u):
        row = jnp.where(gi == 0, ss, u) * rows
        col = jnp.where(gi == 0, tt * UNITS + u, slice_of(ss, tt))
        return full.at[gi, pl.ds(pl.multiple_of(row, rows), rows), lanes(col)]

    def zcopy(gi, b, m, up):
        far = m // UNITS
        at = region(gi, b, (t + 2 * far) % T, m - far * part_units)
        dev = (s + 1) % S if up else (s + S - 1) % S
        return remote(at, at, zss.at[gi, up], zrs.at[gi, b, m], {"sp": dev})

    def xcopy(gi, b, u, tt):
        at = region(gi, b, tt, u)
        return remote(at, at, xss.at[gi], xrs.at[gi, b, u], {"tp": tx})

    def ccopy(gi, b, u, tt):
        at = region(gi, b, tt, u)
        return remote(at, at, css.at[gi], crs.at[gi], {"tp": tc})

    def both_ways(gi, m):
        @pl.when(s + 1 < S)
        def _():
            zcopy(gi, s, m, 1).start()

        @pl.when(s > 0)
        def _():
            zcopy(gi, s, m, 0).start()

    def gather(gi, between, tail):
        for u in range(part_units, UNITS):
            xcopy(gi, s, u, t).start()

        @pl.loop(0, UNITS)
        def _(m):
            both_ways(gi, m)

        for u in range(part_units):
            xcopy(gi, s, u, t).start()

        @pl.loop(0, UNITS)
        def _(u):
            ccopy(gi, s, u, t).start()

        between()

        @pl.loop(0, part_units)
        def _(i):
            xcopy(gi, s, part_units + i, tx).wait_recv()
            both_ways(gi, UNITS + i)
            ccopy(gi, s, part_units + i, tx).start()

        def hop(b, up, m):
            far = m // UNITS
            u = m - far * part_units
            zcopy(gi, b, m, up).wait_recv()

            @pl.when((s + 1 < S) if up else (s > 0))
            def _():
                zcopy(gi, b, m, up).start()

            @pl.when(m < part_units)
            def _():
                xcopy(gi, b, u, t).start()

            ccopy(gi, b, u, (t + 2 * far) % T).start()

        def across(b):
            @pl.when(jnp.logical_and(b >= 0, b < S))
            def _():
                for u in range(part_units):
                    xcopy(gi, b, u, tx).wait_recv()
                    ccopy(gi, b, u, tx).start()

        @pl.loop(1, S)
        def _(d):
            @pl.loop(0, units)
            def _(m):
                @pl.when(s - d >= 0)
                def _():
                    hop(s - d, 1, m)

                @pl.when(s + d < S)
                def _():
                    hop(s + d, 0, m)

            across(s - d + 1)

            @pl.when(d > 1)
            def _():
                across(s + d - 1)

        tail()
        across(s - S + 1)
        across(s + S - 1)
        bulk(full.at[gi, :, pl.ds(0, D // 2)], crs.at[gi])

    def gather_drain(gi):
        for k in range(S - 1):

            @pl.when(s == k)
            def _():
                bulk(full.at[gi, pl.ds(0, 2 * rows), pl.ds(0, (k + 1) * units * LANES // 2)], zss.at[gi, 1])

            @pl.when(s == S - 1 - k)
            def _():
                bulk(full.at[gi, pl.ds(0, 2 * rows), pl.ds(0, (k + 1) * units * LANES // 2)], zss.at[gi, 0])

        bulk(full.at[gi, pl.ds(0, rows), pl.ds(0, (S + 1) * part_units * LANES)], xss.at[gi])
        bulk(full.at[gi, :, pl.ds(0, D // 2)], css.at[gi])

    place = full.at[
        0,
        pl.ds(pl.multiple_of(s * rows, rows), rows),
        pl.ds(pl.multiple_of(t * tcols, tcols), tcols),
    ]
    own = pltpu.make_async_copy(tok_ref, place, lsem.at[0])
    own.start()
    tapb[c] = taps_ref[...]
    logb[c] = logit_ref[...]
    pcopies = [
        remote(ref, buf.at[c], pss.at[i], prs.at[i], {"tp": tc})
        for i, (ref, buf) in enumerate(((taps_ref, tapb), (logit_ref, logb)))
    ]
    for copy in pcopies:
        copy.start()
    weights_start(0, (0, 1))
    weights_start(0, (2,))
    for copy in pcopies:
        copy.wait()
    own.wait()
    depth = S * 2 * half
    step = 64

    def first_half(layer, gi):
        @pl.loop(0, tokens // step)
        def _(i):
            at = pl.ds(pl.multiple_of(i * step, step), step)
            wide = full[gi, at, :].astype(F32)
            scale = lax.rsqrt(jnp.mean(wide * wide, axis=1, keepdims=True) + EPS)
            normed[at, :] = (wide * scale * gain_ref[pl.ds(layer, 1), :]).astype(BF16)

        weights_wait(layer, 0)

        @pl.loop(0, tokens // TILE)
        def _(i):
            at = pl.ds(pl.multiple_of(i * TILE, TILE), TILE)
            proj[at, :] = jnp.dot(
                normed[at, :],
                wbuf[layer].reshape(depth, 2 * LANES),
                preferred_element_type=F32,
            )

        par = tapb[home % 2, layer, :, lanes(sub)]
        rates = jax.nn.softplus(-logb[home % 2, layer, :, lanes(sub)])
        edge = jnp.zeros((8, LANES), F32)
        padded[0:8, :] = edge
        padded[tokens + 8 : tokens + 16, :] = edge
        padded[8 : tokens + 8, :] = proj[:, :LANES].astype(BF16).astype(F32)
        conv = par[0:1] * padded[6 : 6 + tokens, :]
        for k in range(1, TAPS):
            conv = conv + par[k : k + 1] * padded[6 + k : 6 + k + tokens, :]
        convb[layer, c] = conv.astype(BF16)
        vcopy = remote(
            convb.at[layer, c], convb.at[layer, c], vss.at[layer], vrs.at[layer], {"tp": tc}
        )
        vcopy.start()
        weights_forward(layer, 1)
        weights_forward(layer, 2)
        gin = proj[:, LANES:].astype(BF16).astype(F32)
        proj[:, LANES:] = jax.nn.gelu(gin)
        weights_wait(layer, 1)
        vcopy.wait()
        both = jnp.concatenate([convb[layer, 0], convb[layer, 1]], axis=1)
        conv32 = convb[layer, c].astype(F32)
        hidden = None
        for d in range(2):
            pair = []
            for k in (2 * d, 2 * d + 1):
                weight = mbuf[layer, k].reshape(HEAD_W, LANES)
                pair.append(jax.nn.sigmoid(jnp.dot(both, weight, preferred_element_type=F32)))
            log_a = -8.0 * pair[0] * rates[d : d + 1]
            drive = jnp.sqrt(one_minus_exp_neg(-2.0 * log_a)) * pair[1] * conv32
            state = scan_rows(jnp.exp(log_a), drive, d == 1)
            hidden = state if hidden is None else hidden + state
        full[gi + 1, :, lanes(mine)] = (proj[:, LANES:] * hidden).astype(BF16)
    def second_half(layer, gi):
        weights_wait(layer, 2)

        @pl.loop(0, tokens // TILE)
        def _(i):
            at = pl.ds(pl.multiple_of(i * TILE, TILE), TILE)
            prod = jnp.dot(
                full[gi, at, :], obuf[layer].reshape(depth, LANES), preferred_element_type=F32
            )
            old = full[gi - 1, at, lanes(mine)]
            full[gi + 1, at, lanes(mine)] = (old.astype(F32) + prod).astype(BF16)

    @pl.loop(0, 2 * LAYERS)
    def _(gi):
        def between():
            @pl.when(gi % 2 == 0)
            def _():
                weights_forward(gi // 2, 0)

        def tail():
            layer = gi // 2
            more = layer + 1 < LAYERS

            @pl.when(gi % 2 == 0)
            def _():
                weights_start(layer, (3,))

            @pl.when(jnp.logical_and(gi % 2 == 0, more))
            def _():
                weights_start(layer + 1, (0, 1))

            @pl.when(jnp.logical_and(gi % 2 == 1, more))
            def _():
                weights_start(layer + 1, (2,))

        gather(gi, between, tail)

        @pl.when(gi % 2 == 0)
        def _():
            first_half(gi // 2, gi)

        @pl.when(gi % 2 == 1)
        def _():
            second_half(gi // 2, gi)

    def fcopy(ss, q, dev):
        src = full.at[2 * LAYERS, pl.ds(pl.multiple_of(ss * rows, rows), rows), lanes(mine)]
        dst = fin.at[:, lanes(q)]
        if dev is None:
            return pltpu.make_async_copy(src, dst, frs.at[q])
        return remote(src, dst, fss.at[ss], frs.at[q], dev)

    for d in range(S):
        ss = (s + d) % S
        same = jnp.logical_and(ss == s, home == t)

        @pl.when(same)
        def _():
            fcopy(ss, sub, None).start()

        @pl.when(jnp.logical_not(same))
        def _():
            fcopy(ss, sub, {"sp": ss, "tp": home}).start()

    for q in range(T):
        fcopy(0, q, None).wait()
    wide = fin[...].astype(F32)
    sums = jnp.broadcast_to(jnp.sum(wide * wide, axis=1, keepdims=True), (rows, LANES))
    ssq[t] = sums.T[0:8]

    def qcopy(source, d):
        return remote(
            ssq.at[source], ssq.at[source], qss.at[d], qrs.at[source], {"tp": (t + d) % T}
        )

    for d in range(1, T):
        qcopy(t, d).start()
    for d in range(1, T):
        qcopy((t + d) % T, d).wait_recv()
    total = ssq[0]
    for i in range(1, T):
        total = total + ssq[i]
    total = jnp.broadcast_to(total[0:1], (LANES, rows)).T[:, 0:1]
    out_ref[...] = (fin[...].astype(F32) * lax.rsqrt(total / D + EPS) * fgain_ref[...]).astype(BF16)

    for gi in range(2 * LAYERS):
        gather_drain(gi)
    for layer in range(LAYERS):
        for k in range(3):
            weights_drain(layer, k)
    for ss in range(S):

        @pl.when(jnp.logical_not(jnp.logical_and(s == ss, home == t)))
        def _():
            fcopy(ss, sub, {"sp": ss, "tp": home}).wait_send()

    for d in range(1, T):
        qcopy(t, d).wait_send()


def fused(mesh):
    S, T = mesh.shape["sp"], mesh.shape["tp"]

    def run(tokens, norm_gain, in_weight, gate_weight, conv_taps, decay_logit, gate_maps, out_weight, final_gain):
        rows, tcols = tokens.shape
        total = rows * S
        half = in_weight.shape[1] // 2
        dma = pltpu.SemaphoreType.DMA
        n = 2 * LAYERS
        vmem = pl.BlockSpec(memory_space=pltpu.VMEM)
        hbm = pl.BlockSpec(memory_space=pl.ANY)

        def body_of(*refs):
            kernel(S, T, *refs)

        return pl.pallas_call(
            body_of,
            out_shape=jax.ShapeDtypeStruct((rows, tcols), BF16),
            in_specs=[hbm, vmem, hbm, hbm, vmem, vmem, hbm, hbm, vmem],
            out_specs=vmem,
            scratch_shapes=[
                pltpu.VMEM((n + 1, total, D), BF16),
                pltpu.VMEM((total, D), BF16),
                pltpu.VMEM((LAYERS, S, 2, half, 2 * LANES), BF16),
                pltpu.VMEM((LAYERS, S, 2, half, LANES), BF16),
                pltpu.VMEM((LAYERS, S, 2, LANES, LANES), BF16),
                pltpu.VMEM((2, LAYERS, TAPS, tcols), F32),
                pltpu.VMEM((2, LAYERS, 2, tcols), F32),
                pltpu.VMEM((total, 2 * LANES), F32),
                pltpu.VMEM((total + 16, LANES), F32),
                pltpu.VMEM((LAYERS, 2, total, LANES), BF16),
                pltpu.VMEM((rows, tcols), BF16),
                pltpu.VMEM((T, 8, rows), F32),
                dma((LAYERS, 3)),
                dma((LAYERS, 3, S)),
                dma((LAYERS, 3)),
                dma((LAYERS, 3)),
                dma((n, 2)),
                dma((n, S, UNITS + UNITS // 2)),
                dma((n,)),
                dma((n, S, UNITS)),
                dma((n,)),
                dma((n,)),
                dma((LAYERS,)),
                dma((LAYERS,)),
                dma((2,)),
                dma((2,)),
                dma((S,)),
                dma((T,)),
                dma((T,)),
                dma((T,)),
                dma((1,)),
            ],
            compiler_params=pltpu.CompilerParams(
                collective_id=0, has_side_effects=True, vmem_limit_bytes=60 * 1024 * 1024
            ),
        )(tokens, norm_gain, in_weight, gate_weight, conv_taps, decay_logit, gate_maps, out_weight, final_gain.reshape(1, tcols))

    return run


def solution(mesh):
    placed = (
        P(("grp", "sp"), "tp"),
        P(),
        P(None, "sp", "tp"),
        P(None, "sp", "tp"),
        P(None, None, "tp"),
        P(None, None, "tp"),
        P(None, "tp", "sp"),
        P(None, "sp", "tp"),
        P("tp"),
    )
    shape = dict(mesh.shape)
    fits = (
        shape["grp"] == 2
        and shape["tp"] == 4
        and shape["sp"] == 4
        and D == shape["sp"] * shape["tp"] * LANES
        and HEAD_W == 2 * LANES
    )
    return jax.shard_map(
        fused(mesh) if fits else body, mesh=mesh, in_specs=placed, out_specs=P(("grp", "sp"), "tp"), check_vma=False
    )
```

profile of v0, /device:TPU:0, one launch (start us, length us, event | category | flops | bytes accessed | tf_op | source)
XLA Modules:
  0.0 115.5 jit_solution(2595639038451081272)
XLA Ops:
  0.0 113.9 %shard_map.91 = bf16[128,512]{1,0:T(8,128)(2,1)} custom-call(bf16[128,512]{1,0:T(8,128)(2,1)} %refs_0_.1, f32[2,2048]{1,0:T(2,128)} %refs_1_.1, bf16[2,512,512]{2,1,0:T(8,128)(2,1)} %refs_2_.1, bf16[2,512,512]{2,1,0:T(8,128)(2,1)} %refs_3_.1, f32[2,4,512]{2,1,0:T(4,128)} %refs_4_.1, f32[2,2,512]{2,1,0:T(2,128)} %refs_5_.1, bf16[2,512,256]{2,1,0:T(8,128)(2,1)} %refs_6_.1, ...), custom_call_target="tpu_custom_call" | custom-call | tf_op jit(solution)/shard_map/pallas_call | solution.py:612
  113.9 1.6 %copy.11 = bf16[128,512]{1,0:T(8,128)(2,1)} copy(bf16[128,512]{1,0:T(8,128)(2,1)} %shard_map.91) | data formatting | bytes 262144
where the time goes:
time: 116 us; the launch traced here: 115 us
  Pallas kernels  114 us (98%)
  local copies, waits for them, and re-layouts  1.57 us (1%)
    pallas_call x1, Pallas kernels, run(): pl.pallas_call(body_of, out_shape=jax.ShapeDtypeStruct((rows, tcols), BF1...  114 us

commit v1 on v0

--- a/solution.py
+++ b/solution.py
@@ -119,6 +119,7 @@
 
 LANES = 128
 UNITS = 4
+IN, GATE, OUT, MAPS = range(4)
 TILE = 256
 BF16 = jnp.bfloat16
 F32 = jnp.float32
@@ -162,7 +163,6 @@
     full,
     normed,
     wbuf,
-    obuf,
     mbuf,
     tapb,
     logb,
@@ -240,73 +240,74 @@
             device_id_type=pl.DeviceIdType.MESH,
         )
 
+    def weights_at(layer, kind):
+        return mbuf.at[layer] if kind == MAPS else wbuf.at[layer, kind]
+
     def wcopy(layer, kind, q, part, source, dev):
-        if kind == 2:
+        if kind == MAPS:
             src = map_ref.at[
                 layer, pl.ds((q // 2) * HEAD_W + part * LANES, LANES), pl.ds((q % 2) * LANES, LANES)
             ]
-            dst = mbuf.at[layer, source, part]
         else:
-            ref = (in_ref, gate_ref, None, outw_ref)[kind]
-            src = ref.at[layer, pl.ds(part * half, half), pl.ds(q * LANES, LANES)]
-            if kind == 3:
-                dst = obuf.at[layer, source, part]
-            else:
-                dst = wbuf.at[layer, source, part, :, pl.ds(kind * LANES, LANES)]
-        k = max(kind - 1, 0)
-        rsem = wrs.at[layer, k, source]
+            src = (in_ref, gate_ref, outw_ref)[kind].at[
+                layer, pl.ds(part * half, half), pl.ds(q * LANES, LANES)
+            ]
+        dst = weights_at(layer, kind).at[source, part]
+        rsem = wrs.at[layer, kind, source]
         if dev is None:
             return pltpu.make_async_copy(src, dst, rsem)
-        return remote(src, dst, wss.at[layer, k], rsem, {"sp": dev[0], "tp": dev[1]})
-
-    def weights_start(layer, kinds):
-        for kind in kinds:
-            for q in range(T):
-                ds, dt = owner(q)
-
-                @pl.when(ds != s)
-                def _():
-                    wcopy(layer, kind, q, g, s, owner(q)).start()
-
-        for kind in kinds:
-            for q in range(T):
-                ds, dt = owner(q)
-
-                @pl.when(jnp.logical_and(ds == s, dt == t))
-                def _():
-                    for part in range(2):
-                        wcopy(layer, kind, q, part, s, None).start()
-
-                @pl.when(jnp.logical_and(ds == s, dt != t))
-                def _():
-                    for part in range(2):
-                        wcopy(layer, kind, q, part, s, owner(q)).start()
+        return remote(src, dst, wss.at[layer, kind], rsem, {"sp": dev[0], "tp": dev[1]})
+
+    def weights_start(layer, kind):
+        for q in range(T):
+            ds, dt = owner(q)
+
+            @pl.when(ds != s)
+            def _():
+                wcopy(layer, kind, q, g, s, owner(q)).start()
+
+            @pl.when(jnp.logical_and(ds == s, dt == t))
+            def _():
+                for part in range(2):
+                    wcopy(layer, kind, q, part, s, None).start()
+
+            @pl.when(jnp.logical_and(ds == s, dt != t))
+            def _():
+                for part in range(2):
+                    wcopy(layer, kind, q, part, s, owner(q)).start()
 
     def bulk(ref, sem):
         pltpu.make_async_copy(ref, ref, sem).wait()
 
-    def forward(layer, k, source):
-        at = (wbuf, mbuf, obuf)[k].at[layer, source, g]
-        return remote(at, at, yss.at[layer, k], yrs.at[layer, k], {"grp": 1 - g})
-
-    def weights_forward(layer, k):
-        buf = (wbuf, mbuf, obuf)[k]
-        for d in (1, S - 1, *range(2, S - 1)):
-            source = (s + d) % S
-            bulk(buf.at[layer, source, g], wrs.at[layer, k, source])
-            forward(layer, k, source).start()
-
-    def weights_wait(layer, k):
-        buf = (wbuf, mbuf, obuf)[k]
-        bulk(buf.at[layer, s], wrs.at[layer, k, s])
-        bulk(buf.at[layer, pl.ds(0, S - 1), 1 - g], yrs.at[layer, k])
-
-    def weights_drain(layer, k):
-        buf = (wbuf, mbuf, obuf)[k]
-        bulk(buf.at[layer, pl.ds(0, T // 2)], wss.at[layer, k])
-        bulk(buf.at[layer, pl.ds(0, S - 1), g], yss.at[layer, k])
-
-    part_units = UNITS // 2
+    def forward(layer, kind, source):
+        at = weights_at(layer, kind).at[source, g]
+        return remote(at, at, yss.at[layer, kind], yrs.at[layer, kind], {"grp": 1 - g})
+
+    def weights_forward(layer, kind, d):
+        for source in (s - d, s + d):
+
+            @pl.when(jnp.logical_and(source >= 0, source < S))
+            def _():
+                bulk(weights_at(layer, kind).at[source, g], wrs.at[layer, kind, source])
+                forward(layer, kind, source).start()
+
+    def weights_forward_all(layer, kind):
+        @pl.loop(1, S)
+        def _(d):
+            weights_forward(layer, kind, d)
+
+    def weights_wait(layer, kind):
+        buf = weights_at(layer, kind)
+        bulk(buf.at[s], wrs.at[layer, kind, s])
+        bulk(buf.at[pl.ds(0, S - 1), 1 - g], yrs.at[layer, kind])
+
+    def weights_drain(layer, kind):
+        buf = weights_at(layer, kind)
+        bulk(buf.at[pl.ds(0, T // 2)], wss.at[layer, kind])
+        bulk(buf.at[pl.ds(0, S - 1), g], yss.at[layer, kind])
+
+    part_units = 0
+    late_units = UNITS - part_units
     units = UNITS + part_units
 
     def region(gi, ss, tt, u):
@@ -337,28 +338,27 @@
         def _():
             zcopy(gi, s, m, 0).start()
 
-    def gather(gi, between, tail):
-        for u in range(part_units, UNITS):
+    def gather(gi, hook, tail):
+        for u in range(late_units, UNITS):
             xcopy(gi, s, u, t).start()
 
         @pl.loop(0, UNITS)
         def _(m):
             both_ways(gi, m)
 
-        for u in range(part_units):
+        for u in range(late_units):
             xcopy(gi, s, u, t).start()
 
         @pl.loop(0, UNITS)
         def _(u):
             ccopy(gi, s, u, t).start()
 
-        between()
-
-        @pl.loop(0, part_units)
-        def _(i):
-            xcopy(gi, s, part_units + i, tx).wait_recv()
+        hook(0)
+
+        for i in range(part_units):
+            xcopy(gi, s, late_units + i, tx).wait_recv()
             both_ways(gi, UNITS + i)
-            ccopy(gi, s, part_units + i, tx).start()
+            ccopy(gi, s, late_units + i, tx).start()
 
         def hop(b, up, m):
             far = m // UNITS
@@ -369,7 +369,7 @@
             def _():
                 zcopy(gi, b, m, up).start()
 
-            @pl.when(m < part_units)
+            @pl.when(m < late_units)
             def _():
                 xcopy(gi, b, u, t).start()
 
@@ -378,7 +378,7 @@
         def across(b):
             @pl.when(jnp.logical_and(b >= 0, b < S))
             def _():
-                for u in range(part_units):
+                for u in range(late_units):
                     xcopy(gi, b, u, tx).wait_recv()
                     ccopy(gi, b, u, tx).start()
 
@@ -400,6 +400,8 @@
             def _():
                 across(s + d - 1)
 
+            hook(d)
+
         tail()
         across(s - S + 1)
         across(s + S - 1)
@@ -410,13 +412,13 @@
 
             @pl.when(s == k)
             def _():
-                bulk(full.at[gi, pl.ds(0, 2 * rows), pl.ds(0, (k + 1) * units * LANES // 2)], zss.at[gi, 1])
+                bulk(full.at[gi, pl.ds(0, rows), pl.ds(0, (k + 1) * units * LANES)], zss.at[gi, 1])
 
             @pl.when(s == S - 1 - k)
             def _():
-                bulk(full.at[gi, pl.ds(0, 2 * rows), pl.ds(0, (k + 1) * units * LANES // 2)], zss.at[gi, 0])
-
-        bulk(full.at[gi, pl.ds(0, rows), pl.ds(0, (S + 1) * part_units * LANES)], xss.at[gi])
+                bulk(full.at[gi, pl.ds(0, rows), pl.ds(0, (k + 1) * units * LANES)], zss.at[gi, 0])
+
+        bulk(full.at[gi, pl.ds(0, rows), pl.ds(0, (UNITS + (S - 1) * late_units) * LANES)], xss.at[gi])
         bulk(full.at[gi, :, pl.ds(0, D // 2)], css.at[gi])
 
     place = full.at[
@@ -434,10 +436,6 @@
     ]
     for copy in pcopies:
         copy.start()
-    weights_start(0, (0, 1))
-    weights_start(0, (2,))
-    for copy in pcopies:
-        copy.wait()
     own.wait()
     depth = S * 2 * half
     step = 64
@@ -450,23 +448,26 @@
             scale = lax.rsqrt(jnp.mean(wide * wide, axis=1, keepdims=True) + EPS)
             normed[at, :] = (wide * scale * gain_ref[pl.ds(layer, 1), :]).astype(BF16)
 
-        weights_wait(layer, 0)
+        weights_wait(layer, IN)
 
         @pl.loop(0, tokens // TILE)
         def _(i):
             at = pl.ds(pl.multiple_of(i * TILE, TILE), TILE)
-            proj[at, :] = jnp.dot(
-                normed[at, :],
-                wbuf[layer].reshape(depth, 2 * LANES),
-                preferred_element_type=F32,
+            xin = jnp.dot(
+                normed[at, :], wbuf[layer, IN].reshape(depth, LANES), preferred_element_type=F32
             )
+            padded[pl.ds(pl.multiple_of(i * TILE + 8, 8), TILE), :] = xin.astype(BF16).astype(F32)
+
+        @pl.when(layer == 0)
+        def _():
+            for copy in pcopies:
+                copy.wait()
 
         par = tapb[home % 2, layer, :, lanes(sub)]
         rates = jax.nn.softplus(-logb[home % 2, layer, :, lanes(sub)])
         edge = jnp.zeros((8, LANES), F32)
         padded[0:8, :] = edge
         padded[tokens + 8 : tokens + 16, :] = edge
-        padded[8 : tokens + 8, :] = proj[:, :LANES].astype(BF16).astype(F32)
         conv = par[0:1] * padded[6 : 6 + tokens, :]
         for k in range(1, TAPS):
             conv = conv + par[k : k + 1] * padded[6 + k : 6 + k + tokens, :]
@@ -475,11 +476,9 @@
             convb.at[layer, c], convb.at[layer, c], vss.at[layer], vrs.at[layer], {"tp": tc}
         )
         vcopy.start()
-        weights_forward(layer, 1)
-        weights_forward(layer, 2)
-        gin = proj[:, LANES:].astype(BF16).astype(F32)
-        proj[:, LANES:] = jax.nn.gelu(gin)
-        weights_wait(layer, 1)
+        weights_forward_all(layer, MAPS)
+        weights_forward_all(layer, OUT)
+        weights_wait(layer, MAPS)
         vcopy.wait()
         both = jnp.concatenate([convb[layer, 0], convb[layer, 1]], axis=1)
         conv32 = convb[layer, c].astype(F32)
@@ -493,43 +492,70 @@
             drive = jnp.sqrt(one_minus_exp_neg(-2.0 * log_a)) * pair[1] * conv32
             state = scan_rows(jnp.exp(log_a), drive, d == 1)
             hidden = state if hidden is None else hidden + state
-        full[gi + 1, :, lanes(mine)] = (proj[:, LANES:] * hidden).astype(BF16)
+            pass
+        proj[...] = hidden
+        weights_wait(layer, GATE)
+
+        @pl.loop(0, tokens // TILE)
+        def _(i):
+            at = pl.ds(pl.multiple_of(i * TILE, TILE), TILE)
+            gin = jnp.dot(
+                normed[at, :], wbuf[layer, GATE].reshape(depth, LANES), preferred_element_type=F32
+            )
+            gin = gin.astype(BF16).astype(F32)
+            full[gi + 1, at, lanes(mine)] = (jax.nn.gelu(gin) * proj[at, :]).astype(BF16)
+
     def second_half(layer, gi):
-        weights_wait(layer, 2)
+        weights_wait(layer, OUT)
 
         @pl.loop(0, tokens // TILE)
         def _(i):
             at = pl.ds(pl.multiple_of(i * TILE, TILE), TILE)
             prod = jnp.dot(
-                full[gi, at, :], obuf[layer].reshape(depth, LANES), preferred_element_type=F32
+                full[gi, at, :], wbuf[layer, OUT].reshape(depth, LANES), preferred_element_type=F32
             )
             old = full[gi - 1, at, lanes(mine)]
             full[gi + 1, at, lanes(mine)] = (old.astype(F32) + prod).astype(BF16)
 
     @pl.loop(0, 2 * LAYERS)
     def _(gi):
-        def between():
+        layer = gi // 2
+        more = layer + 1 < LAYERS
+
+        def hook(d):
             @pl.when(gi % 2 == 0)
             def _():
-                weights_forward(gi // 2, 0)
+                if isinstance(d, int):
+                    @pl.when(gi == 0)
+                    def _():
+                        weights_start(layer, IN)
+                    @pl.when(gi == 0)
+                    def _():
+                        weights_start(layer, GATE)
+                else:
+                    @pl.when(jnp.logical_and(gi == 0, d == 2))
+                    def _():
+                        weights_start(layer, MAPS)
+                    weights_forward(layer, IN, d)
+                    weights_forward(layer, GATE, d)
+
+            @pl.when(gi % 2 == 1)
+            def _():
+                pass
 
         def tail():
-            layer = gi // 2
-            more = layer + 1 < LAYERS
-
             @pl.when(gi % 2 == 0)
             def _():
-                weights_start(layer, (3,))
-
+                weights_start(layer, OUT)
             @pl.when(jnp.logical_and(gi % 2 == 0, more))
             def _():
-                weights_start(layer + 1, (0, 1))
-
+                weights_start(layer + 1, IN)
+                weights_start(layer + 1, GATE)
             @pl.when(jnp.logical_and(gi % 2 == 1, more))
             def _():
-                weights_start(layer + 1, (2,))
-
-        gather(gi, between, tail)
+                weights_start(layer + 1, MAPS)
+
+        gather(gi, hook, tail)
 
         @pl.when(gi % 2 == 0)
         def _():
@@ -582,8 +608,8 @@
     for gi in range(2 * LAYERS):
         gather_drain(gi)
     for layer in range(LAYERS):
-        for k in range(3):
-            weights_drain(layer, k)
+        for kind in range(4):
+            weights_drain(layer, kind)
     for ss in range(S):
 
         @pl.when(jnp.logical_not(jnp.logical_and(s == ss, home == t)))
@@ -617,22 +643,21 @@
             scratch_shapes=[
                 pltpu.VMEM((n + 1, total, D), BF16),
                 pltpu.VMEM((total, D), BF16),
-                pltpu.VMEM((LAYERS, S, 2, half, 2 * LANES), BF16),
-                pltpu.VMEM((LAYERS, S, 2, half, LANES), BF16),
+                pltpu.VMEM((LAYERS, 3, S, 2, half, LANES), BF16),
                 pltpu.VMEM((LAYERS, S, 2, LANES, LANES), BF16),
                 pltpu.VMEM((2, LAYERS, TAPS, tcols), F32),
                 pltpu.VMEM((2, LAYERS, 2, tcols), F32),
-                pltpu.VMEM((total, 2 * LANES), F32),
+                pltpu.VMEM((total, LANES), F32),
                 pltpu.VMEM((total + 16, LANES), F32),
                 pltpu.VMEM((LAYERS, 2, total, LANES), BF16),
                 pltpu.VMEM((rows, tcols), BF16),
                 pltpu.VMEM((T, 8, rows), F32),
-                dma((LAYERS, 3)),
-                dma((LAYERS, 3, S)),
-                dma((LAYERS, 3)),
-                dma((LAYERS, 3)),
+                dma((LAYERS, 4)),
+                dma((LAYERS, 4, S)),
+                dma((LAYERS, 4)),
+                dma((LAYERS, 4)),
                 dma((n, 2)),
-                dma((n, S, UNITS + UNITS // 2)),
+                dma((n, S, UNITS + 1)),
                 dma((n,)),
                 dma((n, S, UNITS)),
                 dma((n,)),

time: 116 us -> 112 us (0.966)
  Pallas kernels: 114 us -> 110 us
    pallas_call x1, Pallas kernels: 114 us -> 110 us  [run(): pl.pallas_call(body_of, out_shape=jax.ShapeDtypeStruct((rows, tcols), BF1...]
where the time goes in v1:
time: 112 us
  Pallas kernels  110 us (98%)
  local copies, waits for them, and re-layouts  1.57 us (1%)
    pallas_call x1, Pallas kernels, run(): pl.pallas_call(body_of, out_shape=jax.ShapeDtypeStruct((rows, tcols), BF1...  110 us

profile of v1, /device:TPU:0, one launch (start us, length us, event | category | flops | bytes accessed | tf_op | source)
XLA Modules:
  0.0 111.7 jit_solution(2333889849985485996)
XLA Ops:
  0.0 110.2 %shard_map.91 = bf16[128,512]{1,0:T(8,128)(2,1)} custom-call(bf16[128,512]{1,0:T(8,128)(2,1)} %refs_0_.1, f32[2,2048]{1,0:T(2,128)} %refs_1_.1, bf16[2,512,512]{2,1,0:T(8,128)(2,1)} %refs_2_.1, bf16[2,512,512]{2,1,0:T(8,128)(2,1)} %refs_3_.1, f32[2,4,512]{2,1,0:T(4,128)} %refs_4_.1, f32[2,2,512]{2,1,0:T(2,128)} %refs_5_.1, bf16[2,512,256]{2,1,0:T(8,128)(2,1)} %refs_6_.1, ...), custom_call_target="tpu_custom_call" | custom-call | tf_op jit(solution)/shard_map/pallas_call | solution.py:638
  110.2 1.6 %copy.11 = bf16[128,512]{1,0:T(8,128)(2,1)} copy(bf16[128,512]{1,0:T(8,128)(2,1)} %shard_map.91) | data formatting | bytes 262144

commit v2 on v1

v2 whole, which is shorter than its diff:
```python
import jax
import jax.numpy as jnp
from jax import lax
from jax.experimental import pallas as pl
from jax.experimental.pallas import tpu as pltpu
from jax.sharding import PartitionSpec as P

D = 2048
HEAD_W = 256
TAPS = 4
LAYERS = 2


EPS = 1e-06


def extended(value, sides, width):
    for axis, dim in sides:
        devices, length = (lax.axis_size(axis), value.shape[dim])
        up = [(i, (i + 1) % devices) for i in range(devices - 1)]
        down = [(j, i) for i, j in up]
        last = lax.slice_in_dim(value, length - width, length, axis=dim)
        leading = lax.slice_in_dim(value, 0, width, axis=dim)
        before = lax.ppermute(last, axis, up)
        after = lax.ppermute(leading, axis, down)
        value = jnp.concatenate([before, value, after], axis=dim)
    return value


def combine_pair(earlier, later):
    return (earlier[0] * later[0], later[0] * earlier[1] + later[1])


def body(
    tokens,
    norm_gain,
    in_weight,
    gate_weight,
    conv_taps,
    decay_logit,
    gate_maps,
    out_weight,
    final_gain,
):
    resid = tokens
    rows = tokens.shape[0]
    width = in_weight.shape[2]
    local_heads = width // HEAD_W
    for layer in range(LAYERS):
        whole = lax.all_gather(resid, "tp", axis=1, tiled=True)
        wide = whole.astype(jnp.float32)
        normed = (
            wide * lax.rsqrt(jnp.mean(wide * wide, axis=1, keepdims=True) + EPS) * norm_gain[layer]
        ).astype(jnp.bfloat16)
        proj_in = jnp.dot(
            normed,
            lax.all_gather(in_weight[layer], "sp", axis=0, tiled=True),
            preferred_element_type=jnp.float32,
        )
        proj_gate = jnp.dot(
            normed,
            lax.all_gather(gate_weight[layer], "sp", axis=0, tiled=True),
            preferred_element_type=jnp.float32,
        )
        xin = proj_in.astype(jnp.bfloat16)
        gin = proj_gate.astype(jnp.bfloat16)
        padded = extended(xin, (("sp", 0),), 2).astype(jnp.float32)
        conv = conv_taps[layer, 0] * padded[0:rows]
        for k in range(1, TAPS):
            conv = conv + conv_taps[layer, k] * padded[k : k + rows]
        conv = conv.astype(jnp.bfloat16)
        stacked = conv.reshape(rows, local_heads, HEAD_W)
        piece = lax.all_gather(gate_maps[layer], "sp", axis=1, tiled=True)
        blocks = piece.reshape(local_heads, HEAD_W, piece.shape[1])
        pre = jnp.einsum("thi,hij->thj", stacked, blocks, preferred_element_type=jnp.float32)
        pre = pre.reshape(rows, local_heads, 4, HEAD_W)
        conv32 = conv.astype(jnp.float32)
        locals_a = []
        locals_h = []
        for direction in range(2):
            rate = jax.nn.sigmoid(pre[:, :, 2 * direction]).reshape(rows, width)
            inp = jax.nn.sigmoid(pre[:, :, 2 * direction + 1]).reshape(rows, width)
            log_a = -8.0 * rate * jax.nn.softplus(-decay_logit[layer, direction])
            decay = jnp.exp(log_a)
            drive = jnp.sqrt(-jnp.expm1(2.0 * log_a)) * inp * conv32
            prod_a, state = lax.associative_scan(
                combine_pair, (decay, drive), reverse=direction == 1, axis=0
            )
            locals_a.append(prod_a)
            locals_h.append(state)
        summary = jnp.stack([locals_a[0][-1], locals_h[0][-1], locals_a[1][0], locals_h[1][0]])[
            None
        ]
        every = lax.all_gather(summary, "sp", axis=0, tiled=True)
        count = every.shape[0]
        me = lax.axis_index("sp")
        _, incl_f = lax.associative_scan(combine_pair, (every[:, 0], every[:, 1]), axis=0)
        _, incl_b = lax.associative_scan(
            combine_pair, (every[:, 2], every[:, 3]), reverse=True, axis=0
        )
        before = lax.dynamic_index_in_dim(incl_f, jnp.maximum(me - 1, 0), 0, keepdims=False)
        after = lax.dynamic_index_in_dim(incl_b, jnp.minimum(me + 1, count - 1), 0, keepdims=False)
        carry_f = before * (me > 0).astype(jnp.float32)
        carry_b = after * (me < count - 1).astype(jnp.float32)
        hidden = locals_h[0] + locals_a[0] * carry_f + locals_h[1] + locals_a[1] * carry_b
        mix = (jax.nn.gelu(gin.astype(jnp.float32)) * hidden).astype(jnp.bfloat16)
        full_mix = lax.all_gather(mix, "tp", axis=1, tiled=True)
        out = jnp.dot(
            full_mix,
            lax.all_gather(out_weight[layer], "sp", axis=0, tiled=True),
            preferred_element_type=jnp.float32,
        )
        resid = (resid.astype(jnp.float32) + out).astype(jnp.bfloat16)
    wide = resid.astype(jnp.float32)
    total = lax.psum(jnp.sum(wide * wide, axis=1), "tp")
    scale = lax.rsqrt(total / D + EPS)
    return (wide * scale[:, None] * final_gain).astype(jnp.bfloat16)


LANES = 128
IN, GATE, OUT, MAPS = range(4)
BF16 = jnp.bfloat16
F32 = jnp.float32


def shifted(value, k, fill, reverse):
    pad = jnp.full((k, value.shape[1]), fill, value.dtype)
    if reverse:
        return jnp.concatenate([value[k:], pad], axis=0)
    return jnp.concatenate([pad, value[:-k]], axis=0)


def scan_rows(decay, state, reverse):
    k, rows = 1, decay.shape[0]
    while k < rows:
        state = state + decay * shifted(state, k, 0.0, reverse)
        if 2 * k < rows:
            decay = decay * shifted(decay, k, 1.0, reverse)
        k *= 2
    return state


def one_minus_exp_neg(u):
    series = u * (1 - u / 2 * (1 - u / 3 * (1 - u / 4 * (1 - u / 5 * (1 - u / 6 * (1 - u / 7))))))
    return jnp.where(u < 0.3, series, 1.0 - jnp.exp(-u))


def kernel(
    S,
    T,
    tok_ref,
    gain_ref,
    in_ref,
    gate_ref,
    taps_ref,
    logit_ref,
    map_ref,
    outw_ref,
    fgain_ref,
    out_ref,
    full,
    tokb,
    xg,
    wbuf,
    mbuf,
    tapb,
    logb,
    ownb,
    part,
    peer,
    ssq,
    scaleb,
    padded,
    convb,
    hid,
    last,
    sfin,
    ssqf,
    fin,
    ws,
    wr,
    ys,
    yr,
    us,
    ur,
    cs,
    cr,
    ps,
    pr,
    rs,
    rr,
    vss,
    vrs,
    pss,
    prs,
    fss,
    frs,
    qss,
    qrs,
    lsem,
):
    g = lax.axis_index("grp")
    s = lax.axis_index("sp")
    t = lax.axis_index("tp")
    x, c = t // 2, t % 2
    hf, zl = s // 2, s % 2
    sz = s + 1 - 2 * zl
    sp = (s + 2) % S
    tx = (t + 2) % T
    tc = t + 1 - 2 * c
    rows, tcols = tok_ref.shape
    tokens = rows * S
    depth = full.shape[2]
    block = 2 * hf + x
    sub = 2 * zl + c
    mine = T * x + sub
    holder = x == hf

    def lanes(i, n=1):
        return pl.ds(pl.multiple_of(i * LANES, LANES), n * LANES)

    def rows_at(b):
        return pl.ds(pl.multiple_of(b * rows, rows), rows)

    def remote(src, dst, ssem, rsem, dev):
        return pltpu.make_async_remote_copy(
            src_ref=src,
            dst_ref=dst,
            send_sem=ssem,
            recv_sem=rsem,
            device_id=dev,
            device_id_type=pl.DeviceIdType.MESH,
        )

    def bulk(ref, sem):
        pltpu.make_async_copy(ref, ref, sem).wait()

    def both(a, b):
        return jnp.logical_and(a, b)

    barrier = pltpu.get_barrier_semaphore()
    for ds in range(S):
        for dt in range(T):
            if ds or dt:
                pl.semaphore_signal(
                    barrier,
                    inc=1,
                    device_id={"sp": (s + ds) % S, "tp": (t + dt) % T},
                    device_id_type=pl.DeviceIdType.MESH,
                )

    pl.semaphore_signal(
        barrier, inc=1, device_id={"grp": 1 - g}, device_id_type=pl.DeviceIdType.MESH
    )

    piece = lanes(T * c, T)
    own_full = pltpu.make_async_copy(tok_ref, full.at[0, rows_at(s), piece], lsem.at[0])
    own_side = pltpu.make_async_copy(tok_ref, tokb, lsem.at[0])

    @pl.when(holder)
    def _():
        own_full.start()

    @pl.when(jnp.logical_not(holder))
    def _():
        own_side.start()

    pl.semaphore_wait(barrier, S * T)

    def param_copies(k):
        dev = {"tp": 2 * c + k}
        return [
            remote(ref, buf, pss.at[i, k], prs.at[i], dev)
            for i, (ref, buf) in enumerate(((taps_ref, tapb), (logit_ref, logb)))
        ]

    for k in range(2):

        @pl.when(both(holder, 2 * c + k != t))
        def _():
            for copy in param_copies(k):
                copy.start()

    @pl.when(block == t)
    def _():
        tapb[...] = taps_ref[...]
        logb[...] = logit_ref[...]

    def params_wait():
        @pl.when(block != t)
        def _():
            for copy in param_copies(0):
                copy.wait_recv()

    half = in_ref.shape[1] // 2

    def segment(layer, kind, i, part):
        if kind == MAPS:
            return mbuf.at[layer, i, part]
        return wbuf.at[layer, kind, i // 2, part, :, lanes(i % 2)]

    def wcopy(layer, kind, q, part, local):
        if kind == MAPS:
            src = map_ref.at[
                layer, pl.ds((q // 2) * HEAD_W + part * LANES, LANES), pl.ds((q % 2) * LANES, LANES)
            ]
            i, plane = s, 2 * x + q // 2
        else:
            src = (in_ref, gate_ref, outw_ref)[kind].at[
                layer, pl.ds(part * half, half), pl.ds(q * LANES, LANES)
            ]
            i, plane = 2 * zl + jnp.where(holder, 0, 1), 2 * hf + q // 2
        dst = segment(layer, kind, i, part)
        if local:
            return pltpu.make_async_copy(src, dst, wr.at[layer, kind, i])
        dev = {"sp": plane, "tp": 2 * c + q % 2}
        return remote(src, dst, ws.at[layer, kind], wr.at[layer, kind, i], dev)

    def weights_start(layer, kind):
        for q in range(T):
            chip = both(x == c, q // 2 == zl)
            if kind == MAPS:
                chip = both(chip, holder)

            @pl.when(jnp.logical_not(chip))
            def _():
                wcopy(layer, kind, q, g, False).start()

            @pl.when(both(chip, q % 2 == c))
            def _():
                for part in range(2):
                    wcopy(layer, kind, q, part, True).start()

            @pl.when(both(chip, q % 2 != c))
            def _():
                for part in range(2):
                    wcopy(layer, kind, q, part, False).start()

    def near(kind, i):
        if kind == MAPS:
            return both(holder, i == s)
        return i == 2 * zl + jnp.where(holder, 0, 1)

    def passing(layer, kind, i):
        at = segment(layer, kind, i, g)
        return remote(at, at, ys.at[layer, kind], yr.at[layer, kind], {"grp": 1 - g})

    def weights_forward(layer, kind):
        for i in range(4):

            @pl.when(jnp.logical_not(near(kind, i)))
            def _():
                bulk(segment(layer, kind, i, g), wr.at[layer, kind, i])
                passing(layer, kind, i).start()

    def passed(layer, kind, sem):
        deep = LANES if kind == MAPS else half
        if kind != MAPS:
            bulk(full.at[0, pl.ds(0, deep), pl.ds(0, 3 * LANES)], sem)
            return
        for n in (3, 4):

            @pl.when(holder if n == 3 else jnp.logical_not(holder))
            def _():
                bulk(full.at[0, pl.ds(0, deep), pl.ds(0, n * LANES)], sem)

    def weights_wait(layer, kind):
        for i in range(4):

            @pl.when(near(kind, i))
            def _():
                at = mbuf.at[layer, i] if kind == MAPS else wbuf.at[layer, kind, i // 2, :, :, lanes(i % 2)]
                bulk(at, wr.at[layer, kind, i])

        passed(layer, kind, yr.at[layer, kind])

    def weights_drain(layer, kind):
        deep = LANES if kind == MAPS else half
        bulk(full.at[0, pl.ds(0, deep), pl.ds(0, T * LANES)], ws.at[layer, kind])
        passed(layer, kind, ys.at[layer, kind])

    def piece_copy(b, dev, rsem, ssem):
        at = full.at[0, rows_at(b), piece]
        return remote(at, at, ssem, rsem, dev)

    def piece_z(b):
        return piece_copy(b, {"sp": sz}, ur.at[0, b, 0], us.at[0])

    def piece_x(b):
        return piece_copy(b, {"tp": tx}, ur.at[0, b, 0], us.at[1])

    def piece_c(b):
        return piece_copy(b, {"tp": tc}, cr.at[0, b], cs.at[0])

    def piece_far():
        return remote(tokb, full.at[0, rows_at(s), piece], us.at[1], ur.at[0, s, 0], {"sp": sp})

    def piece_arrive(i, b):
        @pl.when(jnp.logical_not(both(holder, i == 0)))
        def _():
            piece_z(b).wait_recv()

        @pl.when(i % 2 == 0)
        def _():
            piece_z(b).start()

            @pl.when(holder)
            def _():
                piece_x(b).start()

        piece_c(b).start()

    places = (
        ({"sp": sz}, T * x + 2 * (1 - zl) + c),
        ({"tp": tx}, T * (1 - x) + 2 * zl + c),
        ({"sp": sz, "tp": tx}, T * (1 - x) + 2 * (1 - zl) + c),
    )

    def unit_copy(gi, b, k):
        at = full.at[gi, rows_at(b), lanes(mine)]
        return remote(at, at, us.at[gi + 1], ur.at[gi, b, k], places[k][0])

    def unit_c(gi, b, j):
        at = full.at[gi, rows_at(b), lanes(j)]
        return remote(at, at, cs.at[gi], cr.at[gi, b], {"tp": tc})

    def unit_send(gi, b):
        for k in range(3):
            unit_copy(gi, b, k).start()
        unit_c(gi, b, mine).start()

    def unit_arrive(gi, b):
        for k in range(3):
            unit_copy(gi, b, k).wait_recv()
            unit_c(gi, b, places[k][1]).start()

    def across_wait(gi, b):
        bulk(full.at[gi, rows_at(b), pl.ds(0, T * LANES)], cr.at[gi, b])

    def part_copy(layer, kind, b):
        return remote(
            part.at[layer, kind, rows_at(b)],
            peer.at[layer, kind, rows_at(b)],
            ps.at[layer, kind],
            pr.at[layer, kind, b],
            {"sp": sp},
        )

    def partial(layer, kind, b, value, slot):
        prod = jnp.dot(
            value, wbuf[layer, kind].reshape(depth, 2 * LANES), preferred_element_type=F32
        )
        ownb[slot, rows_at(b), :] = prod[:, :LANES]
        part[layer, kind, rows_at(b), :] = prod[:, LANES:].astype(BF16)
        part_copy(layer, kind, b).start()

    def whole(layer, kind, b, slot):
        return ownb[slot, rows_at(b), :] + peer[layer, kind, rows_at(b), :].astype(F32)

    def row_of(column):
        return jnp.broadcast_to(column, (rows, LANES)).T[0:8]

    def column_of(row):
        return jnp.broadcast_to(row[0:1], (LANES, rows)).T

    def ssq_copy(layer):
        return remote(ssq.at[layer, 0], ssq.at[layer, 1], rs.at[layer], rr.at[layer], {"sp": sp})

    def block_at(layer, i):
        first = (jnp.where(i % 2 == 0, s, sz) + 2 * (i // 2)) % S
        return jnp.where(layer == 0, first, i)

    def in_phase(layer):
        gi = 2 * layer

        @pl.when(layer == 0)
        def _():
            @pl.loop(0, S)
            def _(i):
                piece_arrive(i, block_at(0, i))
                @pl.when(i == 1)
                def _():
                    weights_start(0, GATE)

                @pl.when(i == 2)
                def _():
                    weights_start(0, MAPS)
                    weights_forward(0, IN)

                @pl.when(i == 3)
                def _():
                    weights_forward(0, GATE)
                    weights_start(0, OUT)


        @pl.loop(0, S + 1)
        def _(i):
            @pl.when(both(layer > 0, i < S))
            def _():
                unit_arrive(gi, i)

            @pl.when(i == 1)
            def _():
                weights_wait(layer, IN)

            @pl.when(i > 0)
            def _():
                e = block_at(layer, i - 1)
                across_wait(gi, e)
                wide = full[gi, rows_at(e), :].astype(F32)
                ssq[layer, 0, e] = row_of(jnp.sum(wide * wide, axis=1, keepdims=True))
                gain = gain_ref[pl.ds(layer, 1), pl.ds(pl.multiple_of(hf * depth, depth), depth)]
                xg[rows_at(e), :] = (wide * gain).astype(BF16)
                partial(layer, IN, e, xg[rows_at(e), :], 0)

        ssq_copy(layer).start()
        weights_wait(layer, GATE)

        @pl.loop(0, S)
        def _(b):
            partial(layer, GATE, b, xg[rows_at(b), :], 1)

        weights_forward(layer, MAPS)

        @pl.when(layer + 1 < LAYERS)
        def _():
            weights_start(layer + 1, IN)
            weights_start(layer + 1, GATE)
            weights_start(layer + 1, MAPS)


        @pl.when(layer == 0)
        def _():
            params_wait()

        ssq_copy(layer).wait_recv()

        @pl.loop(0, S)
        def _(b):
            total = column_of(ssq[layer, 0, b] + ssq[layer, 1, b])
            scale = lax.rsqrt(total / D + EPS)
            scaleb[rows_at(b), :] = scale
            part_copy(layer, IN, b).wait_recv()
            xin = (scale * whole(layer, IN, b, 0)).astype(BF16).astype(F32)
            padded[pl.ds(pl.multiple_of(b * rows + 8, 8), rows), :] = xin

    def recurrence(layer):
        par = tapb[layer, :, lanes(sub)]
        rates = jax.nn.softplus(-logb[layer, :, lanes(sub)])
        edge = jnp.zeros((8, LANES), F32)
        padded[0:8, :] = edge
        padded[tokens + 8 : tokens + 16, :] = edge
        conv = par[0:1] * padded[6 : 6 + tokens, :]
        for k in range(1, TAPS):
            conv = conv + par[k : k + 1] * padded[6 + k : 6 + k + tokens, :]
        convb[layer, c] = conv.astype(BF16)
        vcopy = remote(
            convb.at[layer, c], convb.at[layer, c], vss.at[layer], vrs.at[layer], {"tp": tc}
        )
        vcopy.start()
        weights_wait(layer, MAPS)
        vcopy.wait()
        pair_in = jnp.concatenate([convb[layer, 0], convb[layer, 1]], axis=1)
        conv32 = convb[layer, c].astype(F32)
        hidden = None
        for d in range(2):
            pair = []
            for k in (2 * d, 2 * d + 1):
                pair.append(
                    jax.nn.sigmoid(jnp.dot(pair_in, mbuf[layer, k].reshape(HEAD_W, LANES), preferred_element_type=F32))
                )
            log_a = -8.0 * pair[0] * rates[d : d + 1]
            drive = jnp.sqrt(one_minus_exp_neg(-2.0 * log_a)) * pair[1] * conv32
            state = scan_rows(jnp.exp(log_a), drive, d == 1)
            hidden = state if hidden is None else hidden + state
        hid[...] = hidden
        weights_forward(layer, OUT)


        @pl.loop(0, S)
        def _(b):
            part_copy(layer, GATE, b).wait_recv()
            gin = (scaleb[rows_at(b), :] * whole(layer, GATE, b, 1)).astype(BF16).astype(F32)
            mix = (jax.nn.gelu(gin) * hid[rows_at(b), :]).astype(BF16)
            full[2 * layer + 1, rows_at(b), lanes(mine)] = mix
            unit_send(2 * layer + 1, b)

    def fcopy(b, local):
        src = last.at[rows_at(b)]
        dst = fin.at[:, lanes(sub)]
        if local:
            return pltpu.make_async_copy(src, dst, frs.at[0])
        return remote(src, dst, fss.at[b], frs.at[0], {"sp": b, "tp": block})

    def qcopy(b, dt):
        return remote(
            sfin.at[b], ssqf.at[T * s + t], qss.at[b, dt], qrs.at[0], {"sp": b, "tp": dt}
        )

    def final_here(b):
        return both(b == s, block == t)

    def final_send(b):
        @pl.when(final_here(b))
        def _():
            fcopy(b, True).start()

        @pl.when(jnp.logical_not(final_here(b)))
        def _():
            fcopy(b, False).start()

        for dt in range(T):

            @pl.when(both(b == s, t == dt))
            def _():
                ssqf[T * s + t] = sfin[b]

            @pl.when(jnp.logical_not(both(b == s, t == dt)))
            def _():
                qcopy(b, dt).start()

    def out_phase(layer):
        gi = 2 * layer + 1

        @pl.loop(0, S + 1)
        def _(i):
            @pl.when(i < S)
            def _():
                unit_arrive(gi, i)

            @pl.when(i == 1)
            def _():
                weights_wait(layer, OUT)

            @pl.when(i > 0)
            def _():
                across_wait(gi, i - 1)
                partial(layer, OUT, i - 1, full[gi, rows_at(i - 1), :], 0)

        @pl.when(layer + 1 < LAYERS)
        def _():
            weights_forward(layer + 1, IN)
            weights_forward(layer + 1, GATE)
            weights_start(layer + 1, OUT)


        @pl.loop(0, S)
        def _(b):
            part_copy(layer, OUT, b).wait_recv()
            old = full[gi - 1, rows_at(b), lanes(mine)].astype(F32)
            new = (old + whole(layer, OUT, b, 0)).astype(BF16)

            @pl.when(layer + 1 < LAYERS)
            def _():
                full[gi + 1, rows_at(b), lanes(mine)] = new
                unit_send(gi + 1, b)

            @pl.when(layer + 1 == LAYERS)
            def _():
                last[rows_at(b), :] = new
                wide = new.astype(F32)
                sfin[b] = row_of(jnp.sum(wide * wide, axis=1, keepdims=True))
                final_send(b)

    @pl.when(holder)
    def _():
        own_full.wait()

    @pl.when(jnp.logical_not(holder))
    def _():
        own_side.wait()
        piece_far().start()

    weights_start(0, IN)

    @pl.loop(0, LAYERS)
    def _(layer):
        in_phase(layer)
        recurrence(layer)
        out_phase(layer)

    bulk(ssqf.at[pl.ds(0, S * T - 1)], qrs.at[0])
    total = ssqf[0]
    for i in range(1, S * T):
        total = total + ssqf[i]
    total = column_of(total)[:, 0:1]
    bulk(fin, frs.at[0])
    out_ref[...] = (fin[...].astype(F32) * lax.rsqrt(total / D + EPS) * fgain_ref[...]).astype(BF16)

    for k in range(2):

        @pl.when(both(holder, 2 * c + k != t))
        def _():
            for copy in param_copies(k):
                copy.wait_send()

    for layer in range(LAYERS):
        for kind in range(4):
            weights_drain(layer, kind)
        for kind in range(3):
            bulk(part.at[layer, kind], ps.at[layer, kind])
        ssq_copy(layer).wait_send()
    bulk(full.at[0, pl.ds(0, 2 * rows), pl.ds(0, T * LANES)], us.at[0])

    @pl.when(holder)
    def _():
        bulk(full.at[0, pl.ds(0, 2 * rows), pl.ds(0, T * LANES)], us.at[1])

    @pl.when(jnp.logical_not(holder))
    def _():
        bulk(tokb, us.at[1])

    for gi in range(2 * LAYERS):
        bulk(full.at[gi, :, pl.ds(0, T * LANES)], cs.at[gi])
        if gi:
            bulk(full.at[gi, :, pl.ds(0, 3 * LANES)], us.at[gi + 1])
    for b in range(S):

        @pl.when(jnp.logical_not(final_here(b)))
        def _():
            fcopy(b, False).wait_send()

        for dt in range(T):

            @pl.when(jnp.logical_not(both(b == s, t == dt)))
            def _():
                qcopy(b, dt).wait_send()


def fused(mesh):
    S, T = mesh.shape["sp"], mesh.shape["tp"]

    def run(tokens, norm_gain, in_weight, gate_weight, conv_taps, decay_logit, gate_maps, out_weight, final_gain):
        rows, tcols = tokens.shape
        total = rows * S
        depth = D // 2
        dma = pltpu.SemaphoreType.DMA
        n = 2 * LAYERS
        vmem = pl.BlockSpec(memory_space=pltpu.VMEM)
        hbm = pl.BlockSpec(memory_space=pl.ANY)

        def body_of(*refs):
            kernel(S, T, *refs)

        return pl.pallas_call(
            body_of,
            out_shape=jax.ShapeDtypeStruct((rows, tcols), BF16),
            in_specs=[hbm, vmem, hbm, hbm, vmem, vmem, hbm, hbm, vmem],
            out_specs=vmem,
            scratch_shapes=[
                pltpu.VMEM((n, total, depth), BF16),
                pltpu.VMEM((rows, tcols), BF16),
                pltpu.VMEM((total, depth), BF16),
                pltpu.VMEM((LAYERS, 3, 2, 2, in_weight.shape[1] // 2, 2 * LANES), BF16),
                pltpu.VMEM((LAYERS, S, 2, LANES, LANES), BF16),
                pltpu.VMEM((LAYERS, TAPS, tcols), F32),
                pltpu.VMEM((LAYERS, 2, tcols), F32),
                pltpu.VMEM((2, total, LANES), F32),
                pltpu.VMEM((LAYERS, 3, total, LANES), BF16),
                pltpu.VMEM((LAYERS, 3, total, LANES), BF16),
                pltpu.VMEM((LAYERS, 2, S, 8, LANES), F32),
                pltpu.VMEM((total, LANES), F32),
                pltpu.VMEM((total + 16, LANES), F32),
                pltpu.VMEM((LAYERS, 2, total, LANES), BF16),
                pltpu.VMEM((total, LANES), F32),
                pltpu.VMEM((total, LANES), BF16),
                pltpu.VMEM((S, 8, LANES), F32),
                pltpu.VMEM((S * T, 8, LANES), F32),
                pltpu.VMEM((rows, tcols), BF16),
                dma((LAYERS, 4)),
                dma((LAYERS, 4, 4)),
                dma((LAYERS, 4)),
                dma((LAYERS, 4)),
                dma((n + 1,)),
                dma((n, S, 3)),
                dma((n,)),
                dma((n, S)),
                dma((LAYERS, 3)),
                dma((LAYERS, 3, S)),
                dma((LAYERS,)),
                dma((LAYERS,)),
                dma((LAYERS,)),
                dma((LAYERS,)),
                dma((2, 2)),
                dma((2,)),
                dma((S,)),
                dma((1,)),
                dma((S, T)),
                dma((1,)),
                dma((1,)),
            ],
            compiler_params=pltpu.CompilerParams(
                collective_id=0, has_side_effects=True, vmem_limit_bytes=60 * 1024 * 1024
            ),
        )(tokens, norm_gain, in_weight, gate_weight, conv_taps, decay_logit, gate_maps, out_weight, final_gain.reshape(1, tcols))

    return run


def solution(mesh):
    placed = (
        P(("grp", "sp"), "tp"),
        P(),
        P(None, "sp", "tp"),
        P(None, "sp", "tp"),
        P(None, None, "tp"),
        P(None, None, "tp"),
        P(None, "tp", "sp"),
        P(None, "sp", "tp"),
        P("tp"),
    )
    shape = dict(mesh.shape)
    fits = (
        shape["grp"] == 2
        and shape["tp"] == 4
        and shape["sp"] == 4
        and D == shape["sp"] * shape["tp"] * LANES
        and HEAD_W == 2 * LANES
    )
    return jax.shard_map(
        fused(mesh) if fits else body, mesh=mesh, in_specs=placed, out_specs=P(("grp", "sp"), "tp"), check_vma=False
    )
```

time: 112 us -> 103 us (0.920)
  Pallas kernels: 110 us -> 101 us
    pallas_call x1, Pallas kernels: 110 us -> 101 us  [run(): pl.pallas_call(body_of, out_shape=jax.ShapeDtypeStruct((rows, tcols), BF1...]
where the time goes in v2:
time: 103 us
  Pallas kernels  101 us (98%)
  local copies, waits for them, and re-layouts  1.57 us (2%)
    pallas_call x1, Pallas kernels, run(): pl.pallas_call(body_of, out_shape=jax.ShapeDtypeStruct((rows, tcols), BF1...  101 us

profile of v2, /device:TPU:0, one launch (start us, length us, event | category | flops | bytes accessed | tf_op | source)
XLA Modules:
  0.0 102.6 jit_solution(9993557818631406076)
XLA Ops:
  0.0 101.0 %shard_map.91 = bf16[128,512]{1,0:T(8,128)(2,1)} custom-call(bf16[128,512]{1,0:T(8,128)(2,1)} %refs_0_.1, f32[2,2048]{1,0:T(2,128)} %refs_1_.1, bf16[2,512,512]{2,1,0:T(8,128)(2,1)} %refs_2_.1, bf16[2,512,512]{2,1,0:T(8,128)(2,1)} %refs_3_.1, f32[2,4,512]{2,1,0:T(4,128)} %refs_4_.1, f32[2,2,512]{2,1,0:T(2,128)} %refs_5_.1, bf16[2,512,256]{2,1,0:T(8,128)(2,1)} %refs_6_.1, ...), custom_call_target="tpu_custom_call" | custom-call | tf_op jit(solution)/shard_map/pallas_call | solution.py:745
  101.0 1.6 %copy.11 = bf16[128,512]{1,0:T(8,128)(2,1)} copy(bf16[128,512]{1,0:T(8,128)(2,1)} %shard_map.91) | data formatting | bytes 262144

commit v3 on v2

--- a/solution.py
+++ b/solution.py
@@ -163,6 +163,8 @@
     xg,
     wbuf,
     mbuf,
+    gainb,
+    fgainb,
     tapb,
     logb,
     ownb,
@@ -265,6 +267,18 @@
     def _():
         own_side.start()
 
+    gain_copy = pltpu.make_async_copy(
+        gain_ref.at[:, pl.ds(pl.multiple_of(hf * depth, depth), depth)], gainb, lsem.at[1]
+    )
+    gain_copy.start()
+    fgain_copy = pltpu.make_async_copy(fgain_ref, fgainb, lsem.at[2])
+    fgain_copy.start()
+
+    @pl.when(block == t)
+    def _():
+        pltpu.make_async_copy(taps_ref, tapb, prs.at[0]).start()
+        pltpu.make_async_copy(logit_ref, logb, prs.at[1]).start()
+
     pl.semaphore_wait(barrier, S * T)
 
     def param_copies(k):
@@ -281,16 +295,9 @@
             for copy in param_copies(k):
                 copy.start()
 
-    @pl.when(block == t)
-    def _():
-        tapb[...] = taps_ref[...]
-        logb[...] = logit_ref[...]
-
     def params_wait():
-        @pl.when(block != t)
-        def _():
-            for copy in param_copies(0):
-                copy.wait_recv()
+        for copy in param_copies(0):
+            copy.wait_recv()
 
     half = in_ref.shape[1] // 2
 
@@ -392,23 +399,55 @@
     def piece_c(b):
         return piece_copy(b, {"tp": tc}, cr.at[0, b], cs.at[0])
 
-    def piece_far():
-        return remote(tokb, full.at[0, rows_at(s), piece], us.at[1], ur.at[0, s, 0], {"sp": sp})
-
-    def piece_arrive(i, b):
-        @pl.when(jnp.logical_not(both(holder, i == 0)))
-        def _():
-            piece_z(b).wait_recv()
-
-        @pl.when(i % 2 == 0)
-        def _():
-            piece_z(b).start()
-
-            @pl.when(holder)
-            def _():
-                piece_x(b).start()
-
-        piece_c(b).start()
+    hrows = rows // 2
+    side = jnp.where(holder, 0, 1)
+
+    def far_first(h):
+        dev = {"sp": sp, "tp": tx} if h else {"sp": sp}
+        return remote(
+            tokb.at[pl.ds(h * hrows, hrows)],
+            full.at[0, pl.ds(pl.multiple_of(s * rows + h * hrows, hrows), hrows), piece],
+            us.at[1],
+            ur.at[0, s, 0],
+            dev,
+        )
+
+    def far_copy(b, h, k, dev):
+        at = full.at[0, pl.ds(pl.multiple_of(b * rows + h * hrows, hrows), hrows), piece]
+        if k is None:
+            return remote(at, at, cs.at[0], cr.at[0, b], {"tp": tc})
+        return remote(at, at, us.at[2 * LAYERS + 1], ur.at[0, b, k], dev)
+
+    def far_arrive(b, h, k):
+        far_copy(b, h, k, {"sp": sz}).wait_recv()
+        far_copy(b, h, None, None).start()
+
+    def pieces_arrive(hook):
+        @pl.when(jnp.logical_not(holder))
+        def _():
+            piece_z(s).wait_recv()
+
+        piece_z(s).start()
+
+        @pl.when(holder)
+        def _():
+            piece_x(s).start()
+
+        piece_c(s).start()
+        hook(0)
+        far_copy(sp, side, 0, {"sp": sz}).wait_recv()
+        far_copy(sp, side, 1, {"sp": sz, "tp": tx}).start()
+        far_copy(sp, side, 0, {"sp": sz}).start()
+        far_copy(sp, side, 1, {"tp": tx}).start()
+        far_copy(sp, side, None, None).start()
+        hook(1)
+        piece_z(sz).wait_recv()
+        piece_c(sz).start()
+        hook(2)
+        far_arrive(sp, 1 - side, 1)
+        far_arrive((sz + 2) % S, side, 0)
+        far_arrive((sz + 2) % S, 1 - side, 1)
+        hook(3)
 
     places = (
         ({"sp": sz}, T * x + 2 * (1 - zl) + c),
@@ -425,7 +464,7 @@
         return remote(at, at, cs.at[gi], cr.at[gi, b], {"tp": tc})
 
     def unit_send(gi, b):
-        for k in range(3):
+        for k in (2, 0, 1):
             unit_copy(gi, b, k).start()
         unit_c(gi, b, mine).start()
 
@@ -475,23 +514,19 @@
 
         @pl.when(layer == 0)
         def _():
-            @pl.loop(0, S)
-            def _(i):
-                piece_arrive(i, block_at(0, i))
-                @pl.when(i == 1)
-                def _():
+            def hook(i):
+                pass
+                if i == 1:
                     weights_start(0, GATE)
-
-                @pl.when(i == 2)
-                def _():
                     weights_start(0, MAPS)
+                if i == 2:
                     weights_forward(0, IN)
-
-                @pl.when(i == 3)
-                def _():
+                    weights_start(0, OUT)
+                if i == 3:
                     weights_forward(0, GATE)
-                    weights_start(0, OUT)
-
+
+            gain_copy.wait()
+            pieces_arrive(hook)
 
         @pl.loop(0, S + 1)
         def _(i):
@@ -509,11 +544,15 @@
                 across_wait(gi, e)
                 wide = full[gi, rows_at(e), :].astype(F32)
                 ssq[layer, 0, e] = row_of(jnp.sum(wide * wide, axis=1, keepdims=True))
-                gain = gain_ref[pl.ds(layer, 1), pl.ds(pl.multiple_of(hf * depth, depth), depth)]
+                gain = gainb[pl.ds(layer, 1), :]
                 xg[rows_at(e), :] = (wide * gain).astype(BF16)
                 partial(layer, IN, e, xg[rows_at(e), :], 0)
 
         ssq_copy(layer).start()
+        @pl.when(layer == 1)
+        def _():
+            weights_start(layer, OUT)
+
         weights_wait(layer, GATE)
 
         @pl.loop(0, S)
@@ -641,7 +680,6 @@
         def _():
             weights_forward(layer + 1, IN)
             weights_forward(layer + 1, GATE)
-            weights_start(layer + 1, OUT)
 
 
         @pl.loop(0, S)
@@ -669,7 +707,8 @@
     @pl.when(jnp.logical_not(holder))
     def _():
         own_side.wait()
-        piece_far().start()
+        for h in (1, 0):
+            far_first(h).start()
 
     weights_start(0, IN)
 
@@ -685,7 +724,8 @@
         total = total + ssqf[i]
     total = column_of(total)[:, 0:1]
     bulk(fin, frs.at[0])
-    out_ref[...] = (fin[...].astype(F32) * lax.rsqrt(total / D + EPS) * fgain_ref[...]).astype(BF16)
+    fgain_copy.wait()
+    out_ref[...] = (fin[...].astype(F32) * lax.rsqrt(total / D + EPS) * fgainb[...]).astype(BF16)
 
     for k in range(2):
 
@@ -700,16 +740,9 @@
         for kind in range(3):
             bulk(part.at[layer, kind], ps.at[layer, kind])
         ssq_copy(layer).wait_send()
-    bulk(full.at[0, pl.ds(0, 2 * rows), pl.ds(0, T * LANES)], us.at[0])
-
-    @pl.when(holder)
-    def _():
-        bulk(full.at[0, pl.ds(0, 2 * rows), pl.ds(0, T * LANES)], us.at[1])
-
-    @pl.when(jnp.logical_not(holder))
-    def _():
-        bulk(tokb, us.at[1])
-
+    for k in range(2):
+        bulk(tokb, us.at[k])
+    bulk(full.at[0, pl.ds(0, 3 * hrows), pl.ds(0, T * LANES)], us.at[2 * LAYERS + 1])
     for gi in range(2 * LAYERS):
         bulk(full.at[gi, :, pl.ds(0, T * LANES)], cs.at[gi])
         if gi:
@@ -745,7 +778,7 @@
         return pl.pallas_call(
             body_of,
             out_shape=jax.ShapeDtypeStruct((rows, tcols), BF16),
-            in_specs=[hbm, vmem, hbm, hbm, vmem, vmem, hbm, hbm, vmem],
+            in_specs=[hbm] * 9,
             out_specs=vmem,
             scratch_shapes=[
                 pltpu.VMEM((n, total, depth), BF16),
@@ -753,6 +786,8 @@
                 pltpu.VMEM((total, depth), BF16),
                 pltpu.VMEM((LAYERS, 3, 2, 2, in_weight.shape[1] // 2, 2 * LANES), BF16),
                 pltpu.VMEM((LAYERS, S, 2, LANES, LANES), BF16),
+                pltpu.VMEM((LAYERS, depth), F32),
+                pltpu.VMEM((1, tcols), F32),
                 pltpu.VMEM((LAYERS, TAPS, tcols), F32),
                 pltpu.VMEM((LAYERS, 2, tcols), F32),
                 pltpu.VMEM((2, total, LANES), F32),
@@ -771,7 +806,7 @@
                 dma((LAYERS, 4, 4)),
                 dma((LAYERS, 4)),
                 dma((LAYERS, 4)),
-                dma((n + 1,)),
+                dma((n + 2,)),
                 dma((n, S, 3)),
                 dma((n,)),
                 dma((n, S)),
@@ -787,7 +822,7 @@
                 dma((1,)),
                 dma((S, T)),
                 dma((1,)),
-                dma((1,)),
+                dma((3,)),
             ],
             compiler_params=pltpu.CompilerParams(
                 collective_id=0, has_side_effects=True, vmem_limit_bytes=60 * 1024 * 1024

time: 103 us -> 93.7 us (0.910)
  Pallas kernels: 101 us -> 92 us
    pallas_call x1, Pallas kernels: 101 us -> 92 us  [run(): pl.pallas_call(body_of, out_shape=jax.ShapeDtypeStruct((rows, tcols), BF1...]
where the time goes in v3:
time: 93.7 us; the launch traced here: 93.6 us
  Pallas kernels  92 us (98%)
  local copies, waits for them, and re-layouts  1.57 us (2%)
    pallas_call x1, Pallas kernels, run(): pl.pallas_call(body_of, out_shape=jax.ShapeDtypeStruct((rows, tcols), BF1...  92 us

profile of v3, /device:TPU:0, one launch (start us, length us, event | category | flops | bytes accessed | tf_op | source)
XLA Modules:
  0.0 93.6 jit_solution(9031454683916193255)
XLA Ops:
  0.0 92.0 %shard_map.91 = bf16[128,512]{1,0:T(8,128)(2,1)} custom-call(bf16[128,512]{1,0:T(8,128)(2,1)} %refs_0_.1, f32[2,2048]{1,0:T(2,128)} %refs_1_.1, bf16[2,512,512]{2,1,0:T(8,128)(2,1)} %refs_2_.1, bf16[2,512,512]{2,1,0:T(8,128)(2,1)} %refs_3_.1, f32[2,4,512]{2,1,0:T(4,128)} %refs_4_.1, f32[2,2,512]{2,1,0:T(2,128)} %refs_5_.1, bf16[2,512,256]{2,1,0:T(8,128)(2,1)} %refs_6_.1, ...), custom_call_target="tpu_custom_call" | custom-call | tf_op jit(solution)/shard_map/pallas_call | solution.py:778
  92.0 1.6 %copy.11 = bf16[128,512]{1,0:T(8,128)(2,1)} copy(bf16[128,512]{1,0:T(8,128)(2,1)} %shard_map.91) | data formatting | bytes 262144

commit v4 on v3

--- a/solution.py
+++ b/solution.py
@@ -140,9 +140,13 @@
     return state
 
 
-def one_minus_exp_neg(u):
+def sigmoid(v):
+    return 0.5 * jnp.tanh(0.5 * v) + 0.5
+
+
+def one_minus_square(u, decay):
     series = u * (1 - u / 2 * (1 - u / 3 * (1 - u / 4 * (1 - u / 5 * (1 - u / 6 * (1 - u / 7))))))
-    return jnp.where(u < 0.3, series, 1.0 - jnp.exp(-u))
+    return jnp.where(u < 0.3, series, 1.0 - decay * decay)
 
 
 def kernel(
@@ -543,10 +547,10 @@
                 e = block_at(layer, i - 1)
                 across_wait(gi, e)
                 wide = full[gi, rows_at(e), :].astype(F32)
-                ssq[layer, 0, e] = row_of(jnp.sum(wide * wide, axis=1, keepdims=True))
                 gain = gainb[pl.ds(layer, 1), :]
                 xg[rows_at(e), :] = (wide * gain).astype(BF16)
                 partial(layer, IN, e, xg[rows_at(e), :], 0)
+                ssq[layer, 0, e] = row_of(jnp.sum(wide * wide, axis=1, keepdims=True))
 
         ssq_copy(layer).start()
         @pl.when(layer == 1)
@@ -566,6 +570,10 @@
             weights_start(layer + 1, IN)
             weights_start(layer + 1, GATE)
             weights_start(layer + 1, MAPS)
+
+        @pl.when(layer == 0)
+        def _():
+            weights_forward(0, OUT)
 
 
         @pl.when(layer == 0)
@@ -606,14 +614,17 @@
             pair = []
             for k in (2 * d, 2 * d + 1):
                 pair.append(
-                    jax.nn.sigmoid(jnp.dot(pair_in, mbuf[layer, k].reshape(HEAD_W, LANES), preferred_element_type=F32))
+                    sigmoid(jnp.dot(pair_in, mbuf[layer, k].reshape(HEAD_W, LANES), preferred_element_type=F32))
                 )
             log_a = -8.0 * pair[0] * rates[d : d + 1]
-            drive = jnp.sqrt(one_minus_exp_neg(-2.0 * log_a)) * pair[1] * conv32
-            state = scan_rows(jnp.exp(log_a), drive, d == 1)
+            decay = jnp.exp(log_a)
+            drive = jnp.sqrt(one_minus_square(-2.0 * log_a, decay)) * pair[1] * conv32
+            state = scan_rows(decay, drive, d == 1)
             hidden = state if hidden is None else hidden + state
         hid[...] = hidden
-        weights_forward(layer, OUT)
+        @pl.when(layer == 1)
+        def _():
+            weights_forward(1, OUT)
 
 
         @pl.loop(0, S)

time: 93.7 us -> 93.6 us (level)
  no operation moved by 1% of the time
where the time goes in v4:
time: 93.6 us; the launch traced here: 93.4 us
  Pallas kernels  91.9 us (98%)
  local copies, waits for them, and re-layouts  1.57 us (2%)
    pallas_call x1, Pallas kernels, run(): pl.pallas_call(body_of, out_shape=jax.ShapeDtypeStruct((rows, tcols), BF1...  91.9 us

profile of v4, /device:TPU:0, one launch (start us, length us, event | category | flops | bytes accessed | tf_op | source)
XLA Modules:
  0.0 93.4 jit_solution(18225380451761851310)
XLA Ops:
  0.0 91.9 %shard_map.91 = bf16[128,512]{1,0:T(8,128)(2,1)} custom-call(bf16[128,512]{1,0:T(8,128)(2,1)} %refs_0_.1, f32[2,2048]{1,0:T(2,128)} %refs_1_.1, bf16[2,512,512]{2,1,0:T(8,128)(2,1)} %refs_2_.1, bf16[2,512,512]{2,1,0:T(8,128)(2,1)} %refs_3_.1, f32[2,4,512]{2,1,0:T(4,128)} %refs_4_.1, f32[2,2,512]{2,1,0:T(2,128)} %refs_5_.1, bf16[2,512,256]{2,1,0:T(8,128)(2,1)} %refs_6_.1, ...), custom_call_target="tpu_custom_call" | custom-call | tf_op jit(solution)/shard_map/pallas_call | solution.py:789
  91.9 1.6 %copy.11 = bf16[128,512]{1,0:T(8,128)(2,1)} copy(bf16[128,512]{1,0:T(8,128)(2,1)} %shard_map.91) | data formatting | bytes 262144
